TPU v7x, 32 devices: a whole 2x2x4 slice. The times are simulated.
32 devices in a mesh: grp: 2 (over y), dp: 2 (over x), kv: 4 (over z), tp: 2 (over core).
Axes of the slice: x: 2, y: 2, z: 4, core: 2. Of those that a mesh axis runs over, the one named last changes fastest.
Arguments:
- tokens: bfloat16 [32, 2048], P(('grp', 'dp'), ('kv', 'tp')), parts along dimension 0, may hold values from -24 to 24
- memory: float32 [32, 12, 16384], P(('grp', 'dp', 'kv', 'tp')), parts along dimension 0, may hold values from -3 to 3
- mix_gain: float32 [2048], replicated, may hold values from 0.1 to 1.9
- w_query: bfloat16 [2048, 1536], P(None, ('kv', 'tp')), may hold values from -0.125 to 0.125
- w_key: bfloat16 [2048, 1536], P(None, ('kv', 'tp')), may hold values from -0.125 to 0.125
- w_value: bfloat16 [2048, 1536], P(None, ('kv', 'tp')), may hold values from -0.125 to 0.125
- w_gate: bfloat16 [2048, 1536], P(None, ('kv', 'tp')), may hold values from -0.125 to 0.125
- w_beta: bfloat16 [2048, 12], replicated, may hold values from -0.125 to 0.125
- w_decay: bfloat16 [2048, 12], replicated, may hold values from -0.125 to 0.125
- decay_rate: float32 [12], replicated, may hold values from 0.1 to 3
- decay_bias: float32 [12], replicated, may hold values from -2 to 1
- head_gain: float32 [128], replicated, may hold values from 0.1 to 1.9
- w_out: bfloat16 [1536, 2048], P(None, ('kv', 'tp')), may hold values from -0.15625 to 0.15625
- ffn_gain: float32 [2048], replicated, may hold values from 0.1 to 1.9
- w_up: bfloat16 [2048, 8192], P(None, ('kv', 'tp')), may hold values from -0.125 to 0.125
- w_down: bfloat16 [8192, 2048], P(('kv', 'tp')), may hold values from -0.09375 to 0.09375
Outputs:
- layer_out: bfloat16 [32, 2048], P(('grp', 'dp'), ('kv', 'tp')), parts along dimension 0
- new_memory: float32 [32, 12, 16384], P(('grp', 'dp', 'kv', 'tp')), parts along dimension 0
There are 2 independent parts, one for each index of `grp`. A program takes and returns all parts, laid end to end along the dimension named above; an argument that names none is the same for every part. Nothing has to cross between parts.
All inputs are finite; a program needn't handle non-finite values.
Results may differ from a plain program's by a relative error of at most 0.02.
Values may be sent and summed in bfloat16 or wider, within the bound.
A program may use at most 64 MiB of HBM per device.

v0:
```python
import jax
import jax.numpy as jnp
from jax import lax
from jax.sharding import PartitionSpec as P

epsilon = 1e-06


def shortened(value):
    return jax.tree.map(lambda a: a.astype(jnp.bfloat16) if a.dtype == jnp.float32 else a, value)


def delta_step(queries, keys_in, values, gates, strength, log_decay, memory, head_gain):
    count = queries.shape[0]
    heads = strength.shape[1]
    size = head_gain.shape[0]
    highest = lax.Precision.HIGHEST
    query_wide = queries.astype(jnp.float32).reshape(count, heads, size)
    key_wide = keys_in.astype(jnp.float32).reshape(count, heads, size)
    value_wide = values.astype(jnp.float32).reshape(count, heads, size)
    gate_wide = gates.astype(jnp.float32).reshape(count, heads, size)
    unit_key = key_wide * lax.rsqrt(jnp.sum(key_wide * key_wide, axis=-1, keepdims=True) + epsilon)
    matrix = memory.reshape(count, heads, size, size)
    recall = jnp.einsum("bhk,bhkv->bhv", unit_key, matrix, precision=highest)
    retain = jnp.exp(log_decay)[:, :, None, None]
    scaled = strength[:, :, None]
    erased = matrix - jnp.einsum("bhk,bhv->bhkv", unit_key, scaled * recall, precision=highest)
    written = jnp.einsum("bhk,bhv->bhkv", unit_key, scaled * value_wide, precision=highest)
    updated = retain * erased + written
    readout = jnp.einsum("bhk,bhkv->bhv", query_wide, updated, precision=highest)
    normed = readout * lax.rsqrt(jnp.mean(readout * readout, axis=-1, keepdims=True) + epsilon)
    normed = normed * head_gain * jax.nn.silu(gate_wide)
    return (
        updated.reshape(count, heads, size * size),
        normed.reshape(count, heads * size).astype(jnp.bfloat16),
    )


def per_device(
    tokens,
    memory,
    mix_gain,
    w_query,
    w_key,
    w_value,
    w_gate,
    w_beta,
    w_decay,
    decay_rate,
    decay_bias,
    head_gain,
    w_out,
    ffn_gain,
    w_up,
    w_down,
):
    rows = tokens.shape[0]
    owned = memory.shape[0]
    width = mix_gain.shape[0]
    lane = lax.axis_index(("kv", "tp"))
    own_start = lane * owned
    wide = tokens.astype(jnp.float32)
    head_weights = (w_query, w_key, w_value, w_gate)
    small_weights = (w_beta, w_decay)

    def fold_proj(carry, piece, start):
        mine = lax.dynamic_slice_in_dim(piece, own_start, owned, 0)
        large = tuple(
            (jnp.dot(piece, weight, preferred_element_type=jnp.float32) for weight in head_weights)
        )
        small = tuple(
            (jnp.dot(mine, weight, preferred_element_type=jnp.float32) for weight in small_weights)
        )
        return large + small

    def fold_up(total, piece, start):
        return jnp.dot(piece, w_up, preferred_element_type=jnp.float32)

    def with_squares(inner, gain, carry, piece, start):
        piece_wide = piece.astype(jnp.float32)
        lifted = (piece_wide * gain).astype(jnp.bfloat16)
        return (inner(carry[0], lifted, start), jnp.sum(piece_wide * piece_wide, axis=1))

    proj_init = tuple((jnp.zeros((rows, weight.shape[1]), jnp.float32) for weight in head_weights))
    proj_init = proj_init + tuple(
        (jnp.zeros((owned, weight.shape[1]), jnp.float32) for weight in small_weights)
    )
    row_zeros = jnp.zeros((rows,), jnp.float32)
    folded, total_in = with_squares(
        fold_proj,
        mix_gain,
        (proj_init, row_zeros),
        lax.all_gather(tokens, ("kv", "tp"), axis=1, tiled=True),
        jnp.int32(0),
    )
    scale_in = lax.rsqrt(total_in / width + epsilon)
    sent = tuple(((total * scale_in[:, None]).astype(jnp.bfloat16) for total in folded[:4]))
    scale_own = lax.dynamic_slice_in_dim(scale_in, own_start, owned)[:, None]
    strength = jax.nn.sigmoid(folded[4] * scale_own)
    log_decay = -decay_rate * jax.nn.softplus(folded[5] * scale_own + decay_bias)
    queries, keys_in, values, gates = jax.tree.map(
        lambda part, own: part.astype(own.dtype),
        lax.all_to_all(shortened(sent), ("kv", "tp"), split_axis=0, concat_axis=1, tiled=True),
        sent,
    )
    updated, mixed = delta_step(
        queries, keys_in, values, gates, strength, log_decay, memory, head_gain
    )
    branch = jnp.dot(
        lax.all_gather(mixed, ("kv", "tp"), axis=0, tiled=True),
        w_out,
        preferred_element_type=jnp.float32,
    )
    middle = (wide + branch).astype(jnp.bfloat16)
    middle_wide = middle.astype(jnp.float32)
    up_init = jnp.zeros((rows, w_up.shape[1]), jnp.float32)
    raised, total_mid = with_squares(
        fold_up,
        ffn_gain,
        (up_init, row_zeros),
        lax.all_gather(middle, ("kv", "tp"), axis=1, tiled=True),
        jnp.int32(0),
    )
    scale_mid = lax.rsqrt(total_mid / width + epsilon)[:, None]
    hidden = jnp.square(jax.nn.relu(raised * scale_mid)).astype(jnp.bfloat16)
    terms = jnp.dot(hidden, w_down, preferred_element_type=jnp.float32)
    down = lax.psum_scatter(
        terms.astype(jnp.bfloat16), ("kv", "tp"), scatter_dimension=1, tiled=True
    ).astype(jnp.float32)
    layer_out = (middle_wide + down).astype(jnp.bfloat16)
    return (layer_out, updated)


def solution(mesh):
    placed = (
        P(("grp", "dp"), ("kv", "tp")),
        P(("grp", "dp", "kv", "tp"), None, None),
        P(),
        P(None, ("kv", "tp")),
        P(None, ("kv", "tp")),
        P(None, ("kv", "tp")),
        P(None, ("kv", "tp")),
        P(),
        P(),
        P(),
        P(),
        P(),
        P(None, ("kv", "tp")),
        P(),
        P(None, ("kv", "tp")),
        P(("kv", "tp"), None),
    )
    return jax.shard_map(
        per_device,
        mesh=mesh,
        in_specs=placed,
        out_specs=(P(("grp", "dp"), ("kv", "tp")), P(("grp", "dp", "kv", "tp"), None, None)),
        check_vma=False,
    )
```

profile of v0, /device:TPU:0, one launch (start us, length us, event | category | flops | bytes accessed | tf_op | source)
XLA Modules:
  0.0 142.1 jit_solution(9691909267525715545)
XLA Ops:
  7.2 0.0 copy-start
  7.2 0.0 copy-start.3
  7.2 16.1 %all_gather.9 = bf16[8,2048]{1,0:T(8,128)(2,1)S(1)} all-gather(bf16[8,256]{1,0:T(8,128)(2,1)} %param.16), channel_id=1, replica_groups=mesh['grp'=2,'dp'=2,'kv'=4,'tp'=2] {'kv','tp'}, dimensions={1}, use_global_device_ids=true | all-gather | bytes 36864 | tf_op jit(solution)/shard_map/all_gather | solution.py:93
  23.3 0.8 fusion.20
  24.1 1.4 %fusion.10 = bf16[8,1,192]{2,0,1:T(8,128)(2,1)S(1)} fusion(bf16[8,2048]{1,0:T(8,128)(2,1)S(1)} %get-tuple-element.5, bf16[2048,192]{0,1:T(8,128)(2,1)} %param.20, f32[8]{0:T(128)S(1)} %add_rsqrt_fusion.3), kind=kOutput, calls=%fused_computation.17 | convolution fusion | flops 6294528 | bytes 822304 | tf_op jit(solution)/shard_map/dot_general | solution.py:69
  25.6 0.6 copy.23
  26.2 4.6 %all-to-all-start.1 = ((bf16[8,1,192]{2,1,0:T(2,128)(2,1)}), bf16[8,1,192]{2,1,0:T(2,128)(2,1)S(1)}, u32[]{:S(2)}, u32[]{:S(2)}) async-start(bf16[8,1,192]{2,1,0:T(2,128)(2,1)} %copy.23), calls=%async_computation.1 | async-start | bytes 16384 | tf_op jit(solution)/shard_map/all_to_all | solution.py:103
  30.8 0.6 dynamic_slice.7
  31.4 1.4 %fusion.9 = bf16[8,1,192]{2,0,1:T(8,128)(2,1)S(1)} fusion(bf16[8,2048]{1,0:T(8,128)(2,1)S(1)} %get-tuple-element.5, bf16[2048,192]{0,1:T(8,128)(2,1)} %param.21, f32[8]{0:T(128)S(1)} %add_rsqrt_fusion.3), kind=kOutput, calls=%fused_computation.16 | convolution fusion | flops 6294528 | bytes 822304 | tf_op jit(solution)/shard_map/dot_general | solution.py:69
  32.8 1.5 %fusion.8 = bf16[8,1,192]{2,0,1:T(8,128)(2,1)S(1)} fusion(bf16[8,2048]{1,0:T(8,128)(2,1)S(1)} %get-tuple-element.5, bf16[2048,192]{0,1:T(8,128)(2,1)} %param.22, f32[8]{0:T(128)S(1)} %add_rsqrt_fusion.3), kind=kOutput, calls=%fused_computation.15 | convolution fusion | flops 6294528 | bytes 822304 | tf_op jit(solution)/shard_map/dot_general | solution.py:69
  34.3 1.6 %fusion.16 = f32[12]{0:T(128)S(1)} fusion(bf16[2048,12]{0,1:T(8,128)(2,1)} %param.23, bf16[8,2048]{1,0:T(8,128)(2,1)S(1)} %get-tuple-element.5, s32[]{:T(128)S(6)} %select_n.9, f32[]{:T(128)} %bitcast.2), kind=kOutput, calls=%fused_computation.24 | convolution fusion | flops 49200 | bytes 57400 | tf_op jit(solution)/shard_map/dot_general | solution.py:72
  35.9 1.7 %fusion.45 = f32[12]{0:T(128)S(1)} fusion(f32[12]{0:T(128)} %param.26, bf16[2048,12]{0,1:T(8,128)(2,1)} %param.24, bf16[8,2048]{1,0:T(8,128)(2,1)S(1)} %get-tuple-element.5, s32[]{:T(128)S(6)} %select_n.9, f32[12]{0:T(128)} %param.25, f32[]{:T(128)} %bitcast.2), kind=kOutput, calls=%fused_computation.68 | convolution fusion | flops 49272 | bytes 57496 | tf_op jit(solution)/shard_map/dot_general | solution.py:72
  37.6 1.5 %fusion.11 = bf16[8,1,192]{2,0,1:T(8,128)(2,1)S(1)} fusion(bf16[8,2048]{1,0:T(8,128)(2,1)S(1)} %get-tuple-element.5, bf16[2048,192]{0,1:T(8,128)(2,1)} %param.19, f32[8]{0:T(128)S(1)} %add_rsqrt_fusion.3), kind=kOutput, calls=%fused_computation.18 | convolution fusion | flops 6294528 | bytes 822304 | tf_op jit(solution)/shard_map/dot_general | solution.py:69
  39.0 0.6 copy.24
  39.7 0.6 copy.22
  40.3 0.6 copy.25
  40.9 0.0 all-to-all-done.1
  40.9 5.1 %all-to-all-start.3 = ((bf16[8,1,192]{2,1,0:T(2,128)(2,1)}), bf16[8,1,192]{2,1,0:T(2,128)(2,1)S(1)}, u32[]{:S(2)}, u32[]{:S(2)}) async-start(bf16[8,1,192]{2,1,0:T(2,128)(2,1)} %copy.25), calls=%async_computation.3 | async-start | bytes 16384 | tf_op jit(solution)/shard_map/all_to_all | solution.py:103
  46.0 0.1 mul.179
  46.1 0.1 reduce_sum.37
  46.2 0.1 reshape.229
  46.3 0.1 fusion.68
  46.4 5.2 %all-to-all-done.3 = bf16[8,1,192]{2,1,0:T(2,128)(2,1)S(1)} async-done(((bf16[8,1,192]{2,1,0:T(2,128)(2,1)}), bf16[8,1,192]{2,1,0:T(2,128)(2,1)S(1)}, u32[]{:S(2)}, u32[]{:S(2)}) %all-to-all-start.3) | async-done | bytes 3104 | tf_op jit(solution)/shard_map/all_to_all | solution.py:103
  51.6 3.3 %all-to-all-start = ((bf16[8,1,192]{2,1,0:T(2,128)(2,1)}), bf16[8,1,192]{2,1,0:T(2,128)(2,1)S(1)}, u32[]{:S(2)}, u32[]{:S(2)}) async-start(bf16[8,1,192]{2,1,0:T(2,128)(2,1)} %copy.22), calls=%async_computation | async-start | bytes 16384 | tf_op jit(solution)/shard_map/all_to_all | solution.py:103
  54.9 0.1 broadcast_multiply_fusion.1
  55.0 5.5 %all-to-all-done = bf16[8,1,192]{2,1,0:T(2,128)(2,1)S(1)} async-done(((bf16[8,1,192]{2,1,0:T(2,128)(2,1)}), bf16[8,1,192]{2,1,0:T(2,128)(2,1)S(1)}, u32[]{:S(2)}, u32[]{:S(2)}) %all-to-all-start) | async-done | bytes 3104 | tf_op jit(solution)/shard_map/all_to_all | solution.py:103
  60.5 3.3 %all-to-all-start.2 = ((bf16[8,1,192]{2,1,0:T(2,128)(2,1)}), bf16[8,1,192]{2,1,0:T(2,128)(2,1)S(1)}, u32[]{:S(2)}, u32[]{:S(2)}) async-start(bf16[8,1,192]{2,1,0:T(2,128)(2,1)} %copy.24), calls=%async_computation.2 | async-start | bytes 16384 | tf_op jit(solution)/shard_map/all_to_all | solution.py:103
  63.8 0.0 reduce-scatter.2.cloned.1.call-start
  63.9 0.1 reshape.231
  64.0 0.1 reshape.244
  64.1 5.3 %all-to-all-done.2 = bf16[8,1,192]{2,1,0:T(2,128)(2,1)S(1)} async-done(((bf16[8,1,192]{2,1,0:T(2,128)(2,1)}), bf16[8,1,192]{2,1,0:T(2,128)(2,1)S(1)}, u32[]{:S(2)}, u32[]{:S(2)}) %all-to-all-start.2) | async-done | bytes 3104 | tf_op jit(solution)/shard_map/all_to_all | solution.py:103
  69.4 0.1 reshape.230
  69.5 0.8 fusion.38
  70.2 0.1 bitcast_multiply_fusion.2
  70.3 0.3 multiply_add_fusion
  70.6 0.0 copy-start.2
  70.6 0.5 fusion.51
  71.1 0.1 fusion.33
  71.2 0.1 fusion.36
  71.3 14.0 %all-gather = bf16[8,1,1536]{2,1,0:T(2,128)(2,1)S(1)} all-gather(bf16[1,1,1536]{2,1,0:T(2,128)(2,1)S(1)} %reshape.232), channel_id=1, replica_groups=mesh['grp'=2,'dp'=2,'kv'=4,'tp'=2] {'kv','tp'}, dimensions={0}, use_global_device_ids=true | all-gather | bytes 27648 | tf_op jit(solution)/shard_map/all_gather | solution.py:110
  85.3 0.0 copy-done
  85.3 0.2 fusion.7
  85.5 14.1 %all_gather.11 = bf16[8,2048]{1,0:T(8,128)(2,1)S(1)} all-gather(bf16[8,256]{1,0:T(8,128)(2,1)S(1)} %fusion.7), channel_id=1, replica_groups=mesh['grp'=2,'dp'=2,'kv'=4,'tp'=2] {'kv','tp'}, dimensions={1}, use_global_device_ids=true | all-gather | bytes 36864 | tf_op jit(solution)/shard_map/all_gather | solution.py:121
  99.6 0.1 fusion.22
  99.8 5.3 %convolution_convert_fusion = bf16[8,2048]{1,0:T(8,128)(2,1)} fusion(bf16[1024,2048]{1,0:T(8,128)(2,1)} %param.31, bf16[2048,1024]{1,0:T(8,128)(2,1)} %param.30, bf16[8,2048]{1,0:T(8,128)(2,1)S(1)} %all_gather.11, f32[2048]{0:T(1024)S(1)} %copy-done.4, f32[8]{0:T(128)S(1)} %add_rsqrt_fusion), kind=kOutput, calls=%fused_computation | convolution fusion | flops 67207168 | bytes 8462368 | tf_op jit(solution)/shard_map/dot_general | solution.py:126
  105.1 0.0 reduce-scatter.2.cloned.1.call-update
  105.1 28.9 %reduce-scatter.2.cloned.1.call-done = bf16[8,256]{1,0:T(8,128)(2,1)} async-done(((bf16[8,2048]{1,0:T(8,128)(2,1)}), bf16[8,256]{1,0:T(8,128)(2,1)}) %reduce-scatter.2.cloned.1.call-update) | async-done | bytes 4112 | tf_op jit(solution)/shard_map/reduce_scatter | solution.py:127
  134.0 1.3 add_convert_fusion
  (17 shorter events, 0.2 us)
Async XLA Ops:
  7.2 78.2 %copy-start = (bf16[1536,256]{1,0:T(8,128)(2,1)S(1)}, bf16[1536,256]{1,0:T(8,128)(2,1)}, u32[]{:S(2)}) copy-start(bf16[1536,256]{1,0:T(8,128)(2,1)} %param.28) | copy-start | bytes 2359300
  7.2 78.2 %copy-start.3 = (bf16[8,256]{1,0:T(8,128)(2,1)S(1)}, bf16[8,256]{1,0:T(8,128)(2,1)}, u32[]{:S(2)}) copy-start(bf16[8,256]{1,0:T(8,128)(2,1)} %param.16) | copy-start | bytes 12292
  7.2 62.3 %copy-start.1 = (f32[1,12,16384]{2,0,1:T(1,128)S(1)}, f32[1,12,16384]{2,0,1:T(1,128)}, u32[]{:S(2)}) copy-start(f32[1,12,16384]{2,0,1:T(1,128)} %param.17) | copy-start | bytes 2359300
  7.2 64.0 %copy-start.5 = (f32[128]{0:T(128)S(1)}, f32[128]{0:T(128)}, u32[]{:S(2)}) copy-start(f32[128]{0:T(128)} %param.27) | copy-start | bytes 1540
  7.2 92.6 %copy-start.4 = (f32[2048]{0:T(1024)S(1)}, f32[2048]{0:T(1024)}, u32[]{:S(2)}) copy-start(f32[2048]{0:T(1024)} %param.29) | copy-start | bytes 24580
  26.2 14.7 %all-to-all-start.1 = ((bf16[8,1,192]{2,1,0:T(2,128)(2,1)}), bf16[8,1,192]{2,1,0:T(2,128)(2,1)S(1)}, u32[]{:S(2)}, u32[]{:S(2)}) async-start(bf16[8,1,192]{2,1,0:T(2,128)(2,1)} %copy.23), calls=%async_computation.1 | async-start | bytes 16384 | tf_op jit(solution)/shard_map/all_to_all | solution.py:103
  40.9 10.7 %all-to-all-start.3 = ((bf16[8,1,192]{2,1,0:T(2,128)(2,1)}), bf16[8,1,192]{2,1,0:T(2,128)(2,1)S(1)}, u32[]{:S(2)}, u32[]{:S(2)}) async-start(bf16[8,1,192]{2,1,0:T(2,128)(2,1)} %copy.25), calls=%async_computation.3 | async-start | bytes 16384 | tf_op jit(solution)/shard_map/all_to_all | solution.py:103
  51.6 8.9 %all-to-all-start = ((bf16[8,1,192]{2,1,0:T(2,128)(2,1)}), bf16[8,1,192]{2,1,0:T(2,128)(2,1)S(1)}, u32[]{:S(2)}, u32[]{:S(2)}) async-start(bf16[8,1,192]{2,1,0:T(2,128)(2,1)} %copy.22), calls=%async_computation | async-start | bytes 16384 | tf_op jit(solution)/shard_map/all_to_all | solution.py:103
  60.5 8.9 %all-to-all-start.2 = ((bf16[8,1,192]{2,1,0:T(2,128)(2,1)}), bf16[8,1,192]{2,1,0:T(2,128)(2,1)S(1)}, u32[]{:S(2)}, u32[]{:S(2)}) async-start(bf16[8,1,192]{2,1,0:T(2,128)(2,1)} %copy.24), calls=%async_computation.2 | async-start | bytes 16384 | tf_op jit(solution)/shard_map/all_to_all | solution.py:103
  63.8 70.2 %reduce-scatter.2.cloned.1.call-start = ((), (), s32[]{:S(2)}) async-start(), calls=%async_computation.5 | async-start | bytes 36864 | tf_op jit(solution)/shard_map/reduce_scatter | solution.py:127
  70.6 34.5 %copy-start.2 = (f32[12,128,128]{2,1,0:T(8,128)}, f32[12,128,128]{2,1,0:T(8,128)S(1)}, u32[]{:S(2)}) copy-start(f32[12,128,128]{2,1,0:T(8,128)S(1)} %multiply_add_fusion) | copy-start | bytes 2359300
Sparse Core Ops, SparseCore 0:
  105.2 28.7 reduce-scatter.1
where the time goes:
time: 143 us; the launch traced here: 142 us
  waiting for transfers between devices  44.9 us (31%)
  blocking collectives  44.2 us (31%)
  starting transfers between devices  16.4 us (11%)
  matrix products  15.8 us (11%)
  between operations  14.2 us (10%)
  local copies, waits for them, and re-layouts  3.45 us (2%)
  other arithmetic  3.2 us (2%)
    reduce_scatter x1, waiting for transfers between devices, per_device(): lax.psum_scatter(terms.astype(jnp.bfloat16), ('kv', 'tp'), scatter_dimens...  28.9 us
    all_to_all x4, starting transfers between devices, per_device(): lax.all_to_all(shortened(sent), ('kv', 'tp'), split_axis=0, concat_axis=1...  16.4 us
    all_gather x1, blocking collectives, per_device(): lax.all_gather(tokens, ('kv', 'tp'), axis=1, tiled=True)  16.1 us
    all_to_all x4, waiting for transfers between devices, per_device(): lax.all_to_all(shortened(sent), ('kv', 'tp'), split_axis=0, concat_axis=1...  15.9 us
    all_gather x1, blocking collectives, per_device(): lax.all_gather(middle, ('kv', 'tp'), axis=1, tiled=True)  14.1 us
    all_gather x1, blocking collectives, per_device(): lax.all_gather(mixed, ('kv', 'tp'), axis=0, tiled=True)  14 us
    dot_general x4, matrix products, fold_proj(): jnp.dot(piece, weight, preferred_element_type=jnp.float32)  5.79 us
    dot_general x1, matrix products, per_device(): terms = jnp.dot(hidden, w_down, preferred_element_type=jnp.float32)  5.28 us
  transfers between devices with their start and end apart: 5, of which 4 were waited for; matrix products, arithmetic and copies ran while one was open for 8% of the time, Pallas kernels for 0%

commit v1 on v0

v1 whole, which is shorter than its diff:
```python
import functools

import jax
import jax.numpy as jnp
from jax import lax
from jax.experimental import pallas as pl
from jax.experimental.pallas import tpu as pltpu
from jax.sharding import PartitionSpec as P

epsilon = 1e-06
MESH = pl.DeviceIdType.MESH
f32 = jnp.float32
bf16 = jnp.bfloat16


def dot(a, b):
    return jnp.dot(a, b, preferred_element_type=f32)


def column(row):
    h = row.shape[1]
    wide = jnp.broadcast_to(row, (h, h))
    same = lax.broadcasted_iota(jnp.int32, (h, h), 0) == lax.broadcasted_iota(jnp.int32, (h, h), 1)
    return jnp.sum(jnp.where(same, wide, 0.0), axis=1, keepdims=True)


def offsets_of(kvs, tps):
    order = [0]
    for step in range(1, kvs):
        for a in (step, kvs - step):
            if a not in order:
                order.append(a)
    return [(a, b) for a in order for b in range(tps) if (a, b) != (0, 0)]


def kernel(
    kvs,
    tps,
    tokens,
    memory,
    mix_gain,
    w_query,
    w_key,
    w_value,
    w_gate,
    w_beta,
    w_decay,
    decay_rate,
    decay_bias,
    head_gain,
    w_out,
    ffn_gain,
    w_up,
    w_down,
    out,
    new_memory,
    tok_v,
    mem_v,
    mix_v,
    wq_v,
    wk_v,
    wv_v,
    wg_v,
    wb_v,
    wd_v,
    rate_v,
    bias_v,
    hgain_v,
    wout_v,
    fgain_v,
    wup_v,
    wdown_v,
    land_a,
    send_b,
    land_b,
    send_c,
    land_c,
    send_d,
    land_d,
    send_e,
    land_e,
    local_sem,
    send_sem,
    recv_sem,
):
    n = kvs * tps
    rows, w = tok_v.shape
    owned, heads, _ = mem_v.shape
    size = hgain_v.shape[1]
    width = n * w
    kv = lax.axis_index("kv")
    tp = lax.axis_index("tp")
    me = kv * tps + tp
    offsets = offsets_of(kvs, tps)

    def target(offset):
        return {"kv": lax.rem(kv + offset[0], kvs), "tp": lax.rem(tp + offset[1], tps)}

    def lane_of(where):
        return where["kv"] * tps + where["tp"]

    def source(offset):
        return lane_of(
            {"kv": lax.rem(kv + kvs - offset[0], kvs), "tp": lax.rem(tp + tps - offset[1], tps)}
        )

    hbm = (tokens, w_query, w_key, w_value, w_gate, w_beta, w_decay, mix_gain)
    hbm += (decay_rate, decay_bias, head_gain, memory, w_out, ffn_gain, w_up, w_down)
    vmem = (tok_v, wq_v, wk_v, wv_v, wg_v, wb_v, wd_v, mix_v)
    vmem += (rate_v, bias_v, hgain_v, mem_v, wout_v, fgain_v, wup_v, wdown_v)
    loads = [pltpu.make_async_copy(a, b, local_sem.at[i]) for i, (a, b) in enumerate(zip(hbm, vmem))]
    for load in loads:
        load.start()

    barrier = pltpu.get_barrier_semaphore()
    for offset in offsets:
        pl.semaphore_signal(barrier, inc=1, device_id=target(offset), device_id_type=MESH)
    pl.semaphore_wait(barrier, n - 1)

    def exchange(phase, outgoing, landing):
        copies = []
        for i, offset in reversed(list(enumerate(offsets))):
            where = target(offset)
            copy = pltpu.make_async_remote_copy(
                src_ref=outgoing(lane_of(where)),
                dst_ref=landing.at[me],
                send_sem=send_sem.at[phase, i],
                recv_sem=recv_sem.at[phase, i],
                device_id=where,
                device_id_type=MESH,
            )
            copy.start()
            copies.append(copy)
        return copies[::-1]

    loads[0].wait()
    copies_a = exchange(0, lambda lane: tok_v, land_a)
    for load in loads[1:8]:
        load.wait()
    mats = (wq_v, wk_v, wv_v, wg_v, wb_v, wd_v)

    def lift(piece, gain_v, lane):
        wide = piece.astype(f32)
        return (wide * gain_v[lane]).astype(bf16), jnp.sum(wide * wide, axis=1, keepdims=True)

    def project(piece, gain_v, lane, weights):
        lifted, squares = lift(piece, gain_v, lane)
        start = pl.multiple_of(lane * w, w)
        return [dot(lifted, weight[pl.ds(start, w), :]) for weight in weights] + [squares]

    totals = project(tok_v[...], mix_v, me, mats)
    for copy, offset in zip(copies_a, offsets):
        copy.wait_recv()
        src = source(offset)
        terms = project(land_a[src], mix_v, src, mats)
        totals = [a + b for a, b in zip(totals, terms)]
    scale_in = lax.rsqrt(totals[6] / width + epsilon)
    q, k, v, g, beta, decay = [total * scale_in for total in totals[:6]]
    for lane in range(n):
        for o in range(owned):
            r = lane * owned + o
            stacked = jnp.concatenate([x[r : r + 1] for x in (q, k, v, g)], axis=0)
            send_b[lane, o] = stacked.astype(bf16)
    copies_b = exchange(1, lambda lane: send_b.at[lane], land_b)
    land_b[me] = send_b[me]

    for load in loads[8:12]:
        load.wait()
    rate = column(rate_v[...])
    bias = column(bias_v[...])
    row_at = lax.broadcasted_iota(jnp.int32, (rows, heads), 0)
    strengths, retains = [], []
    for o in range(owned):
        mine = row_at == me * owned + o
        own_beta = column(jnp.sum(jnp.where(mine, beta, 0.0), axis=0, keepdims=True))
        own_decay = column(jnp.sum(jnp.where(mine, decay, 0.0), axis=0, keepdims=True))
        strengths.append(jax.nn.sigmoid(own_beta))
        x = own_decay + bias
        softplus = jnp.maximum(x, 0.0) + jnp.log1p(jnp.exp(-jnp.abs(x)))
        retains.append(jnp.exp(-rate * softplus))

    for copy in copies_b:
        copy.wait_recv()
    writes = []
    for o in range(owned):
        flat = jnp.concatenate([land_b[lane, o].astype(f32) for lane in range(n)], axis=1)
        query, key, value, gate = [
            jnp.concatenate([flat[i : i + 1, h * size : (h + 1) * size] for h in range(heads)], axis=0)
            for i in range(4)
        ]
        unit = key * lax.rsqrt(jnp.sum(key * key, axis=1, keepdims=True) + epsilon)
        recalls = [jnp.zeros((heads, size), f32) for _ in range(2)]
        reads = [jnp.zeros((heads, size), f32) for _ in range(2)]
        for i in range(size):
            row = mem_v[o, :, i * size : (i + 1) * size]
            recalls[i % 2] += unit[:, i : i + 1] * row
            reads[i % 2] += query[:, i : i + 1] * row
        recall = recalls[0] + recalls[1]
        read = reads[0] + reads[1]
        update = strengths[o] * (value - retains[o] * recall)
        readout = retains[o] * read + jnp.sum(query * unit, axis=1, keepdims=True) * update
        normed = readout * lax.rsqrt(jnp.mean(readout * readout, axis=1, keepdims=True) + epsilon)
        normed = normed * hgain_v[...] * (gate * jax.nn.sigmoid(gate))
        send_c[o] = normed.astype(bf16)
        writes.append((unit, update))
    copies_c = exchange(2, lambda lane: send_c, land_c)
    land_c[me] = send_c[...]

    for o in range(owned):
        unit, update = writes[o]
        for i in range(size):
            part = slice(i * size, (i + 1) * size)
            new_memory[o, :, part] = retains[o] * mem_v[o, :, part] + unit[:, i : i + 1] * update

    loads[12].wait()
    for copy in copies_c:
        copy.wait_recv()
    blocks = [land_c[lane, o].astype(f32) for lane in range(n) for o in range(owned)]
    mixed = jnp.concatenate(
        [jnp.concatenate([block[h : h + 1] for block in blocks], axis=0) for h in range(heads)], axis=1
    ).astype(bf16)
    branch = dot(mixed, wout_v[...])
    middle = (tok_v[...].astype(f32) + branch).astype(bf16)
    send_d[...] = middle
    copies_d = exchange(3, lambda lane: send_d, land_d)

    for load in loads[13:15]:
        load.wait()
    totals = project(middle, fgain_v, me, (wup_v,))
    for copy, offset in zip(copies_d, offsets):
        copy.wait_recv()
        src = source(offset)
        terms = project(land_d[src], fgain_v, src, (wup_v,))
        totals = [a + b for a, b in zip(totals, terms)]
    scale_mid = lax.rsqrt(totals[1] / width + epsilon)
    hidden = jnp.square(jnp.maximum(totals[0] * scale_mid, 0.0)).astype(bf16)

    loads[15].wait()
    chunk = w if w % 128 == 0 else width
    for first in range(0, width, chunk):
        terms = dot(hidden, wdown_v[:, first : first + chunk]).astype(bf16)
        for c in range(0, chunk, w):
            send_e[(first + c) // w] = terms[:, c : c + w]
    copies_e = exchange(4, lambda lane: send_e.at[lane], land_e)
    down = send_e[me].astype(f32)
    for copy, offset in zip(copies_e, offsets):
        copy.wait_recv()
        down = down + land_e[source(offset)].astype(f32)
    out[...] = (middle.astype(f32) + down).astype(bf16)
    for copies in (copies_a, copies_b, copies_c, copies_d, copies_e):
        for copy in copies:
            copy.wait_send()


def per_device(kvs, tps, *args):
    (tokens, memory, mix_gain, w_query, w_key, w_value, w_gate, w_beta, w_decay) = args[:9]
    (decay_rate, decay_bias, head_gain, w_out, ffn_gain, w_up, w_down) = args[9:]
    n = kvs * tps
    rows, w = tokens.shape
    owned, heads, _ = memory.shape
    size = head_gain.shape[0]
    columns = w_query.shape[1]
    operands = (
        tokens,
        memory,
        mix_gain.reshape(n, 1, w),
        w_query,
        w_key,
        w_value,
        w_gate,
        w_beta,
        w_decay,
        decay_rate.reshape(1, heads),
        decay_bias.reshape(1, heads),
        head_gain.reshape(1, size),
        w_out,
        ffn_gain.reshape(n, 1, w),
        w_up,
        w_down,
    )
    scratch = [pltpu.VMEM(x.shape, x.dtype) for x in operands]
    scratch += [
        pltpu.VMEM((n, rows, w), bf16),
        pltpu.VMEM((n, owned, 4, columns), bf16),
        pltpu.VMEM((n, owned, 4, columns), bf16),
        pltpu.VMEM((owned, heads, size), bf16),
        pltpu.VMEM((n, owned, heads, size), bf16),
        pltpu.VMEM((rows, w), bf16),
        pltpu.VMEM((n, rows, w), bf16),
        pltpu.VMEM((n, rows, w), bf16),
        pltpu.VMEM((n, rows, w), bf16),
        pltpu.SemaphoreType.DMA((len(operands),)),
        pltpu.SemaphoreType.DMA((5, n - 1)),
        pltpu.SemaphoreType.DMA((5, n - 1)),
    ]
    return pl.pallas_call(
        functools.partial(kernel, kvs, tps),
        out_shape=(
            jax.ShapeDtypeStruct((rows, w), bf16),
            jax.ShapeDtypeStruct(memory.shape, f32),
        ),
        in_specs=[pl.BlockSpec(memory_space=pltpu.HBM)] * len(operands),
        out_specs=(
            pl.BlockSpec(memory_space=pltpu.VMEM),
            pl.BlockSpec(memory_space=pltpu.VMEM),
        ),
        scratch_shapes=scratch,
        compiler_params=pltpu.CompilerParams(
            collective_id=0, has_side_effects=True, vmem_limit_bytes=48 * 1024 * 1024
        ),
    )(*operands)


def solution(mesh):
    placed = (
        P(("grp", "dp"), ("kv", "tp")),
        P(("grp", "dp", "kv", "tp"), None, None),
        P(),
        P(None, ("kv", "tp")),
        P(None, ("kv", "tp")),
        P(None, ("kv", "tp")),
        P(None, ("kv", "tp")),
        P(),
        P(),
        P(),
        P(),
        P(),
        P(None, ("kv", "tp")),
        P(),
        P(None, ("kv", "tp")),
        P(("kv", "tp"), None),
    )
    return jax.shard_map(
        functools.partial(per_device, mesh.shape["kv"], mesh.shape["tp"]),
        mesh=mesh,
        in_specs=placed,
        out_specs=(P(("grp", "dp"), ("kv", "tp")), P(("grp", "dp", "kv", "tp"), None, None)),
        check_vma=False,
    )
```

time: 143 us -> 46.2 us (0.32)
  waiting for transfers between devices: 44.9 us -> 0 us
  blocking collectives: 44.2 us -> 0 us
  Pallas kernels: 0 us -> 26.7 us
  starting transfers between devices: 16.4 us -> 0 us
  matrix products: 15.8 us -> 0 us
  local copies, waits for them, and re-layouts: 3.45 us -> 18.3 us
  between operations: 14.2 us -> 0.72 us
  other arithmetic: 3.2 us -> 0 us
    all_gather x3 -> x0, blocking collectives: 44.2 us -> none  [the longest x1 16.1 us: per_device(): lax.all_gather(tokens, ('kv', 'tp'), axis=1, tiled=True)]
    reduce_scatter x1 -> x0, waiting for transfers between devices: 28.9 us -> none  [per_device(): lax.psum_scatter(terms.astype(jnp.bfloat16), ('kv', 'tp'), scatter_dimens...]
    pallas_call x0 -> x1, Pallas kernels: none -> 26.7 us  [per_device(): pl.pallas_call(functools.partial(kernel, kvs, tps), out_shape=(jax.ShapeD...]
    unnamed x13 -> x26, local copies, waits for them, and re-layouts: 0.05 us -> 16.6 us
    all_to_all x4 -> x0, starting transfers between devices: 16.4 us -> none  [per_device(): lax.all_to_all(shortened(sent), ('kv', 'tp'), split_axis=0, concat_axis=1...]
    all_to_all x4 -> x0, waiting for transfers between devices: 15.9 us -> none  [per_device(): lax.all_to_all(shortened(sent), ('kv', 'tp'), split_axis=0, concat_axis=1...]
    dot_general x10 -> x0, matrix products: 15.8 us -> none  [the longest x4 5.79 us: fold_proj(): jnp.dot(piece, weight, preferred_element_type=jnp.float32)]
    all_to_all x4 -> x0, local copies, waits for them, and re-layouts: 2.43 us -> none  [per_device(): lax.all_to_all(shortened(sent), ('kv', 'tp'), split_axis=0, concat_axis=1...]
  transfers between devices with their start and end apart: 5 -> 0, of which waited for: 4 -> 0; matrix products, arithmetic and copies ran while one was open for 8% -> 0% of each run, Pallas kernels for 0% -> 0%
where the time goes in v1:
time: 46.2 us; the launch traced here: 45.7 us
  Pallas kernels  26.7 us (58%)
  local copies, waits for them, and re-layouts  18.3 us (40%)
  between operations  0.72 us (2%)
    pallas_call x1, Pallas kernels, per_device(): pl.pallas_call(functools.partial(kernel, kvs, tps), out_shape=(jax.ShapeD...  26.7 us
    unnamed x26, local copies, waits for them, and re-layouts  16.6 us
    pallas_call x1, local copies, waits for them, and re-layouts, per_device(): pl.pallas_call(functools.partial(kernel, kvs, tps), out_shape=(jax.ShapeD...  1.69 us

profile of v1, /device:TPU:0, one launch (start us, length us, event | category | flops | bytes accessed | tf_op | source)
XLA Modules:
  0.0 45.7 jit_solution(18164508565587973430)
XLA Ops:
  0.6 1.9 %copy.23.w_beta = bf16[2048,12]{1,0:T(8,128)(2,1)} copy(bf16[2048,12]{0,1:T(8,128)(2,1)} %param.23) | data formatting | bytes 98304 | tf_op args[7]
  2.5 1.9 %copy.24.w_decay = bf16[2048,12]{1,0:T(8,128)(2,1)} copy(bf16[2048,12]{0,1:T(8,128)(2,1)} %param.24) | data formatting | bytes 98304 | tf_op args[8]
  4.4 0.0 copy-start.3
  4.4 0.0 copy-start.4
  4.4 0.0 copy-start.5
  4.4 0.0 copy-start.6
  4.4 0.0 copy-start.7
  4.4 0.0 copy-start.8
  4.4 1.7 %copy.18.memory = f32[1,12,16384]{2,1,0:T(8,128)S(1)} copy(f32[1,12,16384]{2,0,1:T(1,128)} %param.17) | data formatting | bytes 1572864 | tf_op args[1]
  6.1 1.4 %copy.19.w_query = bf16[2048,192]{1,0:T(8,128)(2,1)S(1)} copy(bf16[2048,192]{0,1:T(8,128)(2,1)} %param.19) | data formatting | bytes 1572864 | tf_op args[3]
  7.6 1.4 %copy.20.w_key = bf16[2048,192]{1,0:T(8,128)(2,1)S(1)} copy(bf16[2048,192]{0,1:T(8,128)(2,1)} %param.20) | data formatting | bytes 1572864 | tf_op args[4]
  9.0 2.2 %copy.21.w_value = bf16[2048,192]{1,0:T(8,128)(2,1)} copy(bf16[2048,192]{0,1:T(8,128)(2,1)} %param.21) | data formatting | bytes 1572864 | tf_op args[5]
  11.2 2.2 %copy.22.w_gate = bf16[2048,192]{1,0:T(8,128)(2,1)} copy(bf16[2048,192]{0,1:T(8,128)(2,1)} %param.22) | data formatting | bytes 1572864 | tf_op args[6]
  13.4 0.0 copy-done.3
  13.4 0.0 copy-done.4
  13.4 0.0 copy-done.5
  13.4 0.0 copy-done.6
  13.4 0.0 copy-done.7
  13.5 0.0 copy-done.8
  13.5 0.0 copy-start
  13.5 1.0 %copy-done = bf16[2048,12]{1,0:T(8,128)(2,1)S(1)} copy-done((bf16[2048,12]{1,0:T(8,128)(2,1)S(1)}, bf16[2048,12]{1,0:T(8,128)(2,1)}, u32[]{:S(2)}) %copy-start) | copy-done | bytes 49176
  14.5 0.0 copy-start.1
  14.5 1.0 %copy-done.1 = bf16[2048,12]{1,0:T(8,128)(2,1)S(1)} copy-done((bf16[2048,12]{1,0:T(8,128)(2,1)S(1)}, bf16[2048,12]{1,0:T(8,128)(2,1)}, u32[]{:S(2)}) %copy-start.1) | copy-done | bytes 49176
  15.6 0.0 copy-start.2
  15.6 1.1 %copy-done.2 = bf16[1536,256]{1,0:T(8,128)(2,1)S(1)} copy-done((bf16[1536,256]{1,0:T(8,128)(2,1)S(1)}, bf16[1536,256]{1,0:T(8,128)(2,1)}, u32[]{:S(2)}) %copy-start.2) | copy-done | bytes 786456
  16.7 26.7 %shard_map.167 = (bf16[8,256]{1,0:T(8,128)(2,1)S(1)}, f32[1,12,16384]{2,1,0:T(8,128)S(1)}) custom-call(bf16[8,256]{1,0:T(8,128)(2,1)S(1)} %copy-done.5, f32[1,12,16384]{2,1,0:T(8,128)S(1)} %copy.18.memory, f32[8,1,256]{2,1,0:T(1,128)S(1)} %bitcast.5, bf16[2048,192]{1,0:T(8,128)(2,1)S(1)} %copy.19.w_query, bf16[2048,192]{1,0:T(8,128)(2,1)S(1)} %copy.20.w_key, ...), custom_call_target="tpu_custom_call" | custom-call | tf_op jit(solution)/shard_map/pallas_call | solution.py:296
  43.4 1.7 %copy.25 = f32[1,12,16384]{2,0,1:T(1,128)} copy(f32[1,12,16384]{2,1,0:T(8,128)S(1)} %get-tuple-element.3) | data formatting | bytes 1572864 | tf_op jit(solution)/shard_map/pallas_call | solution.py:296
  45.1 0.6 %copy.27 = bf16[8,256]{1,0:T(8,128)(2,1)} copy(bf16[8,256]{1,0:T(8,128)(2,1)S(1)} %get-tuple-element.6) | data formatting | bytes 8192
Async XLA Ops:
  4.4 9.0 %copy-start.3 = (f32[2048]{0:T(1024)S(1)}, f32[2048]{0:T(1024)}, u32[]{:S(2)}) copy-start(f32[2048]{0:T(1024)} %param.18) | copy-start | bytes 24580
  4.4 9.0 %copy-start.4 = (f32[2048]{0:T(1024)S(1)}, f32[2048]{0:T(1024)}, u32[]{:S(2)}) copy-start(f32[2048]{0:T(1024)} %param.29) | copy-start | bytes 24580
  4.4 9.0 %copy-start.5 = (bf16[8,256]{1,0:T(8,128)(2,1)S(1)}, bf16[8,256]{1,0:T(8,128)(2,1)}, u32[]{:S(2)}) copy-start(bf16[8,256]{1,0:T(8,128)(2,1)} %tokens.1) | copy-start | bytes 12292
  4.4 9.0 %copy-start.6 = (f32[12]{0:T(128)S(1)}, f32[12]{0:T(128)}, u32[]{:S(2)}) copy-start(f32[12]{0:T(128)} %param.25) | copy-start | bytes 148
  4.4 9.0 %copy-start.7 = (f32[12]{0:T(128)S(1)}, f32[12]{0:T(128)}, u32[]{:S(2)}) copy-start(f32[12]{0:T(128)} %param.26) | copy-start | bytes 148
  4.4 9.0 %copy-start.8 = (f32[128]{0:T(128)S(1)}, f32[128]{0:T(128)}, u32[]{:S(2)}) copy-start(f32[128]{0:T(128)} %param.27) | copy-start | bytes 1540
  13.5 1.0 %copy-start = (bf16[2048,12]{1,0:T(8,128)(2,1)S(1)}, bf16[2048,12]{1,0:T(8,128)(2,1)}, u32[]{:S(2)}) copy-start(bf16[2048,12]{1,0:T(8,128)(2,1)} %copy.23.w_beta) | copy-start | bytes 147460
  14.5 1.0 %copy-start.1 = (bf16[2048,12]{1,0:T(8,128)(2,1)S(1)}, bf16[2048,12]{1,0:T(8,128)(2,1)}, u32[]{:S(2)}) copy-start(bf16[2048,12]{1,0:T(8,128)(2,1)} %copy.24.w_decay) | copy-start | bytes 147460
  15.6 1.1 %copy-start.2 = (bf16[1536,256]{1,0:T(8,128)(2,1)S(1)}, bf16[1536,256]{1,0:T(8,128)(2,1)}, u32[]{:S(2)}) copy-start(bf16[1536,256]{1,0:T(8,128)(2,1)} %w_out.1) | copy-start | bytes 2359300

commit v2 on v1

--- a/solution.py
+++ b/solution.py
@@ -15,6 +15,10 @@
 
 def dot(a, b):
     return jnp.dot(a, b, preferred_element_type=f32)
+
+
+def dot_across(a, b):
+    return lax.dot_general(a, b, (((1,), (1,)), ((), ())), preferred_element_type=f32)
 
 
 def column(row):
@@ -85,8 +89,7 @@
 ):
     n = kvs * tps
     rows, w = tok_v.shape
-    owned, heads, _ = mem_v.shape
-    size = hgain_v.shape[1]
+    owned, heads, size, _ = mem_v.shape
     width = n * w
     kv = lax.axis_index("kv")
     tp = lax.axis_index("tp")
@@ -143,17 +146,31 @@
         wide = piece.astype(f32)
         return (wide * gain_v[lane]).astype(bf16), jnp.sum(wide * wide, axis=1, keepdims=True)
 
-    def project(piece, gain_v, lane, weights):
+    def project(piece, gain_v, lane, weights, across):
         lifted, squares = lift(piece, gain_v, lane)
-        start = pl.multiple_of(lane * w, w)
-        return [dot(lifted, weight[pl.ds(start, w), :]) for weight in weights] + [squares]
-
-    totals = project(tok_v[...], mix_v, me, mats)
-    for copy, offset in zip(copies_a, offsets):
-        copy.wait_recv()
-        src = source(offset)
-        terms = project(land_a[src], mix_v, src, mats)
-        totals = [a + b for a, b in zip(totals, terms)]
+        part = pl.ds(pl.multiple_of(lane * w, w), w)
+        if across:
+            return [dot_across(lifted, weight[:, part]) for weight in weights] + [squares]
+        return [dot(lifted, weight[part, :]) for weight in weights] + [squares]
+
+    def project_all(own, landing, copies, gain_v, weights, across):
+        if w % 128 == 0:
+            totals = project(own, gain_v, me, weights, across)
+            for copy, offset in zip(copies, offsets):
+                copy.wait_recv()
+                src = source(offset)
+                terms = project(landing[src], gain_v, src, weights, across)
+                totals = [a + b for a, b in zip(totals, terms)]
+            return totals
+        landing[me] = own
+        for copy in copies:
+            copy.wait_recv()
+        lifts = [lift(landing[lane], gain_v, lane) for lane in range(n)]
+        lifted = jnp.concatenate([a.astype(f32) for a, _ in lifts], axis=1).astype(bf16)
+        squares = sum(b for _, b in lifts)
+        return [(dot_across if across else dot)(lifted, weight[...]) for weight in weights] + [squares]
+
+    totals = project_all(tok_v[...], land_a, copies_a, mix_v, mats, True)
     scale_in = lax.rsqrt(totals[6] / width + epsilon)
     q, k, v, g, beta, decay = [total * scale_in for total in totals[:6]]
     for lane in range(n):
@@ -189,28 +206,30 @@
             for i in range(4)
         ]
         unit = key * lax.rsqrt(jnp.sum(key * key, axis=1, keepdims=True) + epsilon)
-        recalls = [jnp.zeros((heads, size), f32) for _ in range(2)]
-        reads = [jnp.zeros((heads, size), f32) for _ in range(2)]
-        for i in range(size):
-            row = mem_v[o, :, i * size : (i + 1) * size]
-            recalls[i % 2] += unit[:, i : i + 1] * row
-            reads[i % 2] += query[:, i : i + 1] * row
-        recall = recalls[0] + recalls[1]
-        read = reads[0] + reads[1]
+        unit_t, query_t = unit.T, query.T
+        recalls, reads = [], []
+        for h in range(heads):
+            matrix = mem_v[o, h]
+            recalls.append(jnp.sum(unit_t[:, h : h + 1] * matrix, axis=0, keepdims=True))
+            reads.append(jnp.sum(query_t[:, h : h + 1] * matrix, axis=0, keepdims=True))
+        recall = jnp.concatenate(recalls, axis=0)
+        read = jnp.concatenate(reads, axis=0)
         update = strengths[o] * (value - retains[o] * recall)
         readout = retains[o] * read + jnp.sum(query * unit, axis=1, keepdims=True) * update
         normed = readout * lax.rsqrt(jnp.mean(readout * readout, axis=1, keepdims=True) + epsilon)
         normed = normed * hgain_v[...] * (gate * jax.nn.sigmoid(gate))
         send_c[o] = normed.astype(bf16)
-        writes.append((unit, update))
+        writes.append((unit_t, update))
     copies_c = exchange(2, lambda lane: send_c, land_c)
     land_c[me] = send_c[...]
 
     for o in range(owned):
-        unit, update = writes[o]
-        for i in range(size):
-            part = slice(i * size, (i + 1) * size)
-            new_memory[o, :, part] = retains[o] * mem_v[o, :, part] + unit[:, i : i + 1] * update
+        unit_t, update = writes[o]
+        for h in range(heads):
+            kept = retains[o][h : h + 1] * mem_v[o, h]
+            mem_v[o, h] = kept + unit_t[:, h : h + 1] * update[h : h + 1]
+    store = pltpu.make_async_copy(mem_v, new_memory, local_sem.at[len(loads)])
+    store.start()
 
     loads[12].wait()
     for copy in copies_c:
@@ -226,12 +245,7 @@
 
     for load in loads[13:15]:
         load.wait()
-    totals = project(middle, fgain_v, me, (wup_v,))
-    for copy, offset in zip(copies_d, offsets):
-        copy.wait_recv()
-        src = source(offset)
-        terms = project(land_d[src], fgain_v, src, (wup_v,))
-        totals = [a + b for a, b in zip(totals, terms)]
+    totals = project_all(middle, land_d, copies_d, fgain_v, (wup_v,), False)
     scale_mid = lax.rsqrt(totals[1] / width + epsilon)
     hidden = jnp.square(jnp.maximum(totals[0] * scale_mid, 0.0)).astype(bf16)
 
@@ -247,6 +261,7 @@
         copy.wait_recv()
         down = down + land_e[source(offset)].astype(f32)
     out[...] = (middle.astype(f32) + down).astype(bf16)
+    store.wait()
     for copies in (copies_a, copies_b, copies_c, copies_d, copies_e):
         for copy in copies:
             copy.wait_send()
@@ -262,14 +277,14 @@
     columns = w_query.shape[1]
     operands = (
         tokens,
-        memory,
+        memory.reshape(owned, heads, size, size),
         mix_gain.reshape(n, 1, w),
-        w_query,
-        w_key,
-        w_value,
-        w_gate,
-        w_beta,
-        w_decay,
+        w_query.T,
+        w_key.T,
+        w_value.T,
+        w_gate.T,
+        w_beta.T,
+        w_decay.T,
         decay_rate.reshape(1, heads),
         decay_bias.reshape(1, heads),
         head_gain.reshape(1, size),
@@ -289,26 +304,27 @@
         pltpu.VMEM((n, rows, w), bf16),
         pltpu.VMEM((n, rows, w), bf16),
         pltpu.VMEM((n, rows, w), bf16),
-        pltpu.SemaphoreType.DMA((len(operands),)),
+        pltpu.SemaphoreType.DMA((len(operands) + 1,)),
         pltpu.SemaphoreType.DMA((5, n - 1)),
         pltpu.SemaphoreType.DMA((5, n - 1)),
     ]
-    return pl.pallas_call(
+    layer_out, updated = pl.pallas_call(
         functools.partial(kernel, kvs, tps),
         out_shape=(
             jax.ShapeDtypeStruct((rows, w), bf16),
-            jax.ShapeDtypeStruct(memory.shape, f32),
+            jax.ShapeDtypeStruct((owned, heads, size, size), f32),
         ),
         in_specs=[pl.BlockSpec(memory_space=pltpu.HBM)] * len(operands),
         out_specs=(
             pl.BlockSpec(memory_space=pltpu.VMEM),
-            pl.BlockSpec(memory_space=pltpu.VMEM),
+            pl.BlockSpec(memory_space=pltpu.HBM),
         ),
         scratch_shapes=scratch,
         compiler_params=pltpu.CompilerParams(
-            collective_id=0, has_side_effects=True, vmem_limit_bytes=48 * 1024 * 1024
+            collective_id=0, has_side_effects=True, vmem_limit_bytes=65 * 1000 * 1000
         ),
     )(*operands)
+    return layer_out, updated.reshape(memory.shape)
 
 
 def solution(mesh):

time: 46.2 us -> 30.8 us (0.67)
  local copies, waits for them, and re-layouts: 18.3 us -> 3.33 us
    unnamed x26 -> x2, local copies, waits for them, and re-layouts: 16.6 us -> 3.33 us
    pallas_call x1 -> x0, local copies, waits for them, and re-layouts: 1.69 us -> none  [per_device(): pl.pallas_call(functools.partial(kernel, kvs, tps), out_shape=(jax.ShapeD...]
where the time goes in v2:
time: 30.8 us; the launch traced here: 30.6 us
  Pallas kernels  26.6 us (86%)
  local copies, waits for them, and re-layouts  3.33 us (11%)
  between operations  0.65 us (2%)
    pallas_call x1, Pallas kernels, per_device(): pl.pallas_call(functools.partial(kernel, kvs, tps), out_shape=(jax.ShapeD...  26.6 us
    unnamed x2, local copies, waits for them, and re-layouts  3.33 us

profile of v2, /device:TPU:0, one launch (start us, length us, event | category | flops | bytes accessed | tf_op | source)
XLA Modules:
  0.0 30.6 jit_solution(6640939932298517912)
XLA Ops:
  0.6 26.6 %shard_map.167 = (bf16[8,256]{1,0:T(8,128)(2,1)}, f32[1,12,128,128]{3,2,1,0:T(8,128)}) custom-call(bf16[8,256]{1,0:T(8,128)(2,1)} %tokens.1, f32[1,12,128,128]{3,2,1,0:T(8,128)} %bitcast.13, f32[8,1,256]{2,1,0:T(1,128)} %bitcast.21, bf16[192,2048]{1,0:T(8,128)(2,1)} %bitcast.14, bf16[192,2048]{1,0:T(8,128)(2,1)} %bitcast.15, bf16[192,2048]{1,0:T(8,128)(2,1)} %bitcast.16, ...), custom_call_target="tpu_custom_call" | custom-call | tf_op jit(solution)/shard_map/pallas_call | solution.py:311
  27.3 1.3 %copy.21 = bf16[8,256]{1,0:T(8,128)(2,1)} copy(bf16[8,256]{1,0:T(8,128)(2,1)} %get-tuple-element.10) | data formatting | bytes 8192
  28.5 2.1 %copy.22 = f32[1,12,16384]{2,0,1:T(1,128)} copy(f32[1,12,16384]{2,0,1:T(1,128)} %bitcast.18) | data formatting | bytes 1572864

commit v3 on v2

--- a/solution.py
+++ b/solution.py
@@ -112,7 +112,7 @@
     vmem = (tok_v, wq_v, wk_v, wv_v, wg_v, wb_v, wd_v, mix_v)
     vmem += (rate_v, bias_v, hgain_v, mem_v, wout_v, fgain_v, wup_v, wdown_v)
     loads = [pltpu.make_async_copy(a, b, local_sem.at[i]) for i, (a, b) in enumerate(zip(hbm, vmem))]
-    for load in loads:
+    for load in loads[:8]:
         load.start()
 
     barrier = pltpu.get_barrier_semaphore()
@@ -138,35 +138,22 @@
 
     loads[0].wait()
     copies_a = exchange(0, lambda lane: tok_v, land_a)
+    for load in loads[8:]:
+        load.start()
     for load in loads[1:8]:
         load.wait()
     mats = (wq_v, wk_v, wv_v, wg_v, wb_v, wd_v)
 
     def lift(piece, gain_v, lane):
         wide = piece.astype(f32)
-        return (wide * gain_v[lane]).astype(bf16), jnp.sum(wide * wide, axis=1, keepdims=True)
-
-    def project(piece, gain_v, lane, weights, across):
-        lifted, squares = lift(piece, gain_v, lane)
-        part = pl.ds(pl.multiple_of(lane * w, w), w)
-        if across:
-            return [dot_across(lifted, weight[:, part]) for weight in weights] + [squares]
-        return [dot(lifted, weight[part, :]) for weight in weights] + [squares]
+        return wide * gain_v[lane], jnp.sum(wide * wide, axis=1, keepdims=True)
 
     def project_all(own, landing, copies, gain_v, weights, across):
-        if w % 128 == 0:
-            totals = project(own, gain_v, me, weights, across)
-            for copy, offset in zip(copies, offsets):
-                copy.wait_recv()
-                src = source(offset)
-                terms = project(landing[src], gain_v, src, weights, across)
-                totals = [a + b for a, b in zip(totals, terms)]
-            return totals
         landing[me] = own
         for copy in copies:
             copy.wait_recv()
         lifts = [lift(landing[lane], gain_v, lane) for lane in range(n)]
-        lifted = jnp.concatenate([a.astype(f32) for a, _ in lifts], axis=1).astype(bf16)
+        lifted = jnp.concatenate([a for a, _ in lifts], axis=1).astype(bf16)
         squares = sum(b for _, b in lifts)
         return [(dot_across if across else dot)(lifted, weight[...]) for weight in weights] + [squares]
 
@@ -265,6 +252,23 @@
     for copies in (copies_a, copies_b, copies_c, copies_d, copies_e):
         for copy in copies:
             copy.wait_send()
+
+
+def finish(a, b, a_out, b_out, a_v, b_v, sem):
+    owned, heads = b.shape[:2]
+    parts = [(a, a_v, a_out)]
+    for o in range(owned):
+        for h in range(heads):
+            parts.append((b.at[o, h], b_v.at[o, h], b_out.at[o, h]))
+    into = [pltpu.make_async_copy(x, y, sem.at[0, i]) for i, (x, y, _) in enumerate(parts)]
+    back = [pltpu.make_async_copy(y, z, sem.at[1, i]) for i, (_, y, z) in enumerate(parts)]
+    for copy in into:
+        copy.start()
+    for first, second in zip(into, back):
+        first.wait()
+        second.start()
+    for copy in back:
+        copy.wait()
 
 
 def per_device(kvs, tps, *args):
@@ -324,6 +328,21 @@
             collective_id=0, has_side_effects=True, vmem_limit_bytes=65 * 1000 * 1000
         ),
     )(*operands)
+    layer_out, updated = pl.pallas_call(
+        finish,
+        out_shape=(
+            jax.ShapeDtypeStruct(layer_out.shape, layer_out.dtype),
+            jax.ShapeDtypeStruct(updated.shape, updated.dtype),
+        ),
+        in_specs=[pl.BlockSpec(memory_space=pltpu.HBM)] * 2,
+        out_specs=(pl.BlockSpec(memory_space=pltpu.HBM),) * 2,
+        scratch_shapes=[
+            pltpu.VMEM(layer_out.shape, layer_out.dtype),
+            pltpu.VMEM(updated.shape, updated.dtype),
+            pltpu.SemaphoreType.DMA((2, 1 + owned * heads)),
+        ],
+        compiler_params=pltpu.CompilerParams(vmem_limit_bytes=65 * 1000 * 1000),
+    )(layer_out, updated)
     return layer_out, updated.reshape(memory.shape)
 
 

time: 30.8 us -> 29.9 us (0.971)
  local copies, waits for them, and re-layouts: 3.33 us -> 0 us
  Pallas kernels: 26.6 us -> 29 us
    unnamed x2 -> x0, local copies, waits for them, and re-layouts: 3.33 us -> none
    pallas_call x0 -> x1, Pallas kernels: none -> 2.02 us  [per_device(): pl.pallas_call(finish, out_shape=(jax.ShapeDtypeStruct(layer_out.shape, l...]
    pallas_call x1, Pallas kernels: 26.6 us -> 27 us  [per_device(): pl.pallas_call(functools.partial(kernel, kvs, tps), out_shape=(jax.ShapeD...]
where the time goes in v3:
time: 29.9 us; the launch traced here: 29.7 us
  Pallas kernels  29 us (97%)
  between operations  0.64 us (2%)
    pallas_call x1, Pallas kernels, per_device(): pl.pallas_call(functools.partial(kernel, kvs, tps), out_shape=(jax.ShapeD...  27 us
    pallas_call x1, Pallas kernels, per_device(): pl.pallas_call(finish, out_shape=(jax.ShapeDtypeStruct(layer_out.shape, l...  2.02 us

profile of v3, /device:TPU:0, one launch (start us, length us, event | category | flops | bytes accessed | tf_op | source)
XLA Modules:
  0.0 29.7 jit_solution(7274279240840496955)
XLA Ops:
  0.6 27.0 %shard_map.167 = (bf16[8,256]{1,0:T(8,128)(2,1)}, f32[1,12,128,128]{3,2,1,0:T(8,128)}) custom-call(bf16[8,256]{1,0:T(8,128)(2,1)} %tokens.1, f32[1,12,128,128]{3,2,1,0:T(8,128)} %bitcast.13, f32[8,1,256]{2,1,0:T(1,128)} %bitcast.20, bf16[192,2048]{1,0:T(8,128)(2,1)} %bitcast.14, bf16[192,2048]{1,0:T(8,128)(2,1)} %bitcast.15, bf16[192,2048]{1,0:T(8,128)(2,1)} %bitcast.16, ...), custom_call_target="tpu_custom_call" | custom-call | tf_op jit(solution)/shard_map/pallas_call | solution.py:315
  27.6 2.0 %shard_map.168 = (bf16[8,256]{1,0:T(8,128)(2,1)}, f32[1,12,128,128]{3,2,1,0:T(8,128)}) custom-call(bf16[8,256]{1,0:T(8,128)(2,1)} %get-tuple-element.6.a, f32[1,12,128,128]{3,2,1,0:T(8,128)} %get-tuple-element.7.b), custom_call_target="tpu_custom_call" | custom-call | tf_op jit(solution)/shard_map/pallas_call | solution.py:331
